TPU v7x, 512 devices: a whole 4x4x16 slice. The times are simulated.
512 devices in a mesh: sp: 64 (over z, y), tp: 8 (over x, core).
Axes of the slice: x: 4, y: 4, z: 16, core: 2. Of those that a mesh axis runs over, the one named last changes fastest.
Arguments:
- resid: bfloat16 [16384, 2048], P(('sp', 'tp')), may hold values from -6 to 6
- queries: bfloat16 [16384, 1024], P('sp', 'tp'), may hold values from -6 to 6
- keys: bfloat16 [512, 16384], P('tp', 'sp'), may hold values from -6 to 6
- values: bfloat16 [512, 16384], P('tp', 'sp'), may hold values from -6 to 6
- log_gates: float32 [16, 16384], P('tp', 'sp'), may hold values from -1640 to 0, as said below
- q_gain: float32 [64], replicated, may hold values from 0.5 to 7
- k_gain: float32 [64], replicated, may hold values from 0.5 to 7
- w_out: bfloat16 [1024, 2048], P('tp'), may hold values from -0.1875 to 0.1875
- mlp_gain: bfloat16 [2048], replicated, may hold values from 0.099609375 to 1.8984375
- w_up: bfloat16 [2048, 8192], P('sp', 'tp'), may hold values from -0.125 to 0.125
- w_down: bfloat16 [8192, 2048], P('tp', 'sp'), may hold values from -0.0625 to 0.0625
Outputs:
- output: bfloat16 [16384, 2048], P(('sp', 'tp'))
Inputs may be any that keep to these rules, and one draw needn't show every extreme that they name: `log_gates`: each head's values never rise along positions.
All inputs are finite; a program needn't handle non-finite values.
Results may differ from a plain program's by a relative error of at most 0.018.
The roundings to bfloat16 on the way count: a program that leaves them out, or rounds other values in their place, can miss the bound.
Values may be sent and summed in bfloat16 or wider, within the bound.
No kernel may reach another device: no remote copies, remote signals or barrier semaphores. Data moves between devices by JAX's collectives and lax.ppermute only.
A program may use at most 64 MiB of HBM per device.

v0:
```python
import math

import jax
import jax.numpy as jnp
from jax import lax
from jax.sharding import PartitionSpec as P

EPS = 1e-06


def rows_first(arrays, axis, dims):
    turned = [jnp.moveaxis(a, dim, 0) for a, dim in zip(arrays, dims)]
    widths = [t[0].size for t in turned]
    both = jnp.concatenate([t.reshape(-1, w) for t, w in zip(turned, widths)], axis=1)
    result = lax.all_gather(both, axis, axis=0, tiled=True)
    parts = jnp.split(result, [sum(widths[:k]) for k in range(1, len(widths))], axis=1)
    return tuple(
        (
            jnp.moveaxis(b.reshape(-1, *t.shape[1:]), 0, dim)
            for b, t, dim in zip(parts, turned, dims)
        )
    )


def sent_to_all(value, axis):
    count = lax.axis_size(axis)
    return lax.all_to_all(
        jnp.broadcast_to(value[None], (count, *value.shape)), axis, 0, 0, tiled=True
    )


def joined_along(parts, dim):
    lengths = list(parts.shape[1:])
    lengths[dim] *= parts.shape[0]
    return jnp.moveaxis(parts, 0, dim).reshape(lengths)


def gather_directly(value, axis, dim):
    parts = sent_to_all(value, axis)
    return joined_along(parts, dim)


def in_one_piece(arrays, axis, dim, along):
    ends, at = ([], 0)
    for a in arrays[:-1]:
        at += a.shape[along]
        ends.append(at)
    both = jnp.concatenate(arrays, axis=along)
    return tuple(jnp.split(lax.all_gather(both, axis, axis=dim, tiled=True), ends, axis=along))


def cut_along(value, dim, count):
    before, after = (value.shape[:dim], value.shape[dim + 1 :])
    return jnp.moveaxis(value.reshape(*before, count, -1, *after), dim, 0)


def summed_on_arrival(value, axis, dim):
    count = lax.axis_size(axis)
    parts = lax.all_to_all(cut_along(value, dim, count), axis, 0, 0, tiled=True)
    return jnp.sum(parts.astype(jnp.float32), axis=0)


def rms_last(input_values, gain):
    scale = lax.rsqrt(jnp.mean(input_values * input_values, axis=-1, keepdims=True) + EPS)
    return input_values * scale * gain


def local(resid, queries, keys, values, log_gates, q_gain, k_gain, w_out, mlp_gain, w_up, w_down):
    up_whole, down_whole = rows_first((w_up, w_down), "sp", (0, 1))
    positions = queries.shape[0]
    head_size = q_gain.shape[0]
    query_count = log_gates.shape[0]
    key_total_count = keys.shape[0] // head_size
    group = query_count // key_total_count
    query_heads = queries.astype(jnp.float32).reshape(positions, query_count, head_size)
    qnorm = (rms_last(query_heads, q_gain) * head_size ** (-0.5)).astype(jnp.bfloat16)
    qnorm = jnp.transpose(qnorm.reshape(positions, key_total_count, group, head_size), (1, 2, 0, 3))
    key_heads = keys.astype(jnp.float32).reshape(key_total_count, head_size, positions)
    key_scale = lax.rsqrt(jnp.mean(key_heads * key_heads, axis=1, keepdims=True) + EPS)
    knorm = (key_heads * key_scale * k_gain[None, :, None]).astype(jnp.bfloat16)
    knorm = knorm.reshape(key_total_count * head_size, positions)
    gates_all = gather_directly(log_gates, "sp", 1)
    offset = lax.axis_index("sp") * positions
    query_pos = offset + jnp.arange(positions, dtype=jnp.int32)
    query_last = offset + positions - 1
    query_gates = log_gates.reshape(key_total_count, group, positions)
    start_state = (
        jnp.full((key_total_count, group, positions), -1e30, jnp.float32),
        jnp.zeros((key_total_count, group, positions), jnp.float32),
        jnp.zeros((key_total_count, group, positions, head_size), jnp.float32),
    )
    key_piece, value_piece = in_one_piece((knorm, values), "sp", 1, 0)
    length = key_piece.shape[1]
    block = math.gcd(length, 1024)
    key_blocks = key_piece.reshape(key_total_count, head_size, length)
    value_blocks = value_piece.reshape(key_total_count, head_size, length)

    def one_step(index, state):
        first = index * block

        def compute(inner):
            running_top, running_total, running_sum = inner
            key_now = lax.dynamic_slice_in_dim(key_blocks, index * block, block, 2)
            value_now = lax.dynamic_slice_in_dim(value_blocks, index * block, block, 2)
            gates_now = lax.dynamic_slice_in_dim(gates_all, first, block, 1).reshape(
                key_total_count, group, block
            )
            logits = jnp.einsum(
                "kgtd,kdn->kgtn", qnorm, key_now, preferred_element_type=jnp.float32
            )
            logits = logits + query_gates[..., None] - gates_now[:, :, None, :]
            key_pos = first + jnp.arange(block, dtype=jnp.int32)
            logits = jnp.where(key_pos[None, :] <= query_pos[:, None], logits, -jnp.inf)
            new_top = jnp.maximum(running_top, jnp.max(logits, axis=-1))
            rescale = jnp.exp(running_top - new_top)
            weights = jnp.exp(logits - new_top[..., None])
            new_total = running_total * rescale + jnp.sum(weights, axis=-1)
            product = jnp.einsum(
                "kgtn,kdn->kgtd",
                weights.astype(jnp.bfloat16),
                value_now,
                preferred_element_type=jnp.float32,
            )
            return (new_top, new_total, running_sum * rescale[..., None] + product)

        return lax.cond(first <= query_last, compute, lambda inner: inner, state)

    final_top, final_total, final_sum = lax.fori_loop(0, length // block, one_step, start_state)
    attn = final_sum / final_total[..., None]
    attn = (
        jnp.transpose(attn, (2, 0, 1, 3))
        .reshape(positions, query_count * head_size)
        .astype(jnp.bfloat16)
    )
    rows_now = attn
    proj = summed_on_arrival(
        jnp.dot(rows_now, w_out, preferred_element_type=jnp.float32).astype(jnp.bfloat16), "tp", 0
    )
    mixed = (resid.astype(jnp.float32) + proj).astype(jnp.bfloat16)
    normed = rms_last(mixed.astype(jnp.float32), mlp_gain.astype(jnp.float32)).astype(jnp.bfloat16)
    upward = jnp.dot(gather_directly(normed, "tp", 0), up_whole, preferred_element_type=jnp.float32)
    act = jnp.square(jax.nn.relu(upward)).astype(jnp.bfloat16)
    rows_now = act
    summed_down = summed_on_arrival(
        jnp.dot(rows_now, down_whole, preferred_element_type=jnp.float32).astype(jnp.bfloat16),
        "tp",
        0,
    )
    return (mixed.astype(jnp.float32) + summed_down).astype(jnp.bfloat16)


def solution(mesh):
    return jax.shard_map(
        local,
        mesh=mesh,
        in_specs=(
            P(("sp", "tp"), None),
            P("sp", "tp"),
            P("tp", "sp"),
            P("tp", "sp"),
            P("tp", "sp"),
            P(),
            P(),
            P("tp", None),
            P(),
            P("sp", "tp"),
            P("tp", "sp"),
        ),
        out_specs=P(("sp", "tp"), None),
        check_vma=False,
    )
```

profile of v0, /device:TPU:1, one launch (start us, length us, event | category | flops | bytes accessed | tf_op | source)
XLA Modules:
  0.0 348.9 jit_solution(38273085295830202)
XLA Ops:
  6.5 0.0 copy-start
  6.5 0.0 all-gather.3.cloned.1.call-start
  6.5 0.8 fusion.39
  7.4 0.8 fusion.41
  8.2 1.4 pad_maximum_fusion.1
  9.6 0.0 all-gather.3.cloned.1.call-update
  9.6 0.0 all-gather.5.cloned.1.call-start
  9.7 1.5 pad_maximum_fusion
  11.2 0.0 all-gather.5.cloned.1.call-update
  11.3 1.4 broadcast_in_dim.25
  12.6 19.3 %all-to-all-start = ((f32[64,2,256]{2,1,0:T(2,128)}), f32[64,2,256]{2,1,0:T(2,128)S(1)}, u32[]{:S(2)}, u32[]{:S(2)}) async-start(f32[64,2,256]{2,1,0:T(2,128)} %broadcast_in_dim.25), calls=%async_computation | async-start | bytes 262144 | tf_op jit(solution)/shard_map/all_to_all | solution.py:27
  31.9 0.9 copy.17
  32.9 0.7 fusion.42
  33.6 0.0 copy-start.3
  33.7 119.0 %all-gather.3.cloned.1.call-done = bf16[128,16384]{1,0:T(8,128)(2,1)} async-done(((bf16[128,256]{1,0:T(8,128)(2,1)}), bf16[128,16384]{1,0:T(8,128)(2,1)}) %all-gather.3.cloned.1.call-update) | async-done | bytes 4194320 | tf_op jit(solution)/shard_map/all_gather | solution.py:49
  152.6 3.9 %slice_bitcast_fusion = (bf16[1,64,16384]{2,1,0:T(8,128)(2,1)S(1)}, bf16[1,64,16384]{2,1,0:T(8,128)(2,1)}) fusion(bf16[128,16384]{1,0:T(8,128)(2,1)} %all-gather.3.cloned.1.call-done), kind=kLoop, calls=%fused_computation.30 | loop fusion | bytes 8388608 | tf_op jit(solution)/shard_map/reshape | solution.py:96
  156.5 0.0 all-to-all-done
  156.6 0.0 copy-done.3
  156.6 3.4 while.18
  156.6 2.6 conditional.3
  156.7 0.2 broadcast_compare_fusion
  156.9 1.5 fusion.44
  158.4 0.5 fusion.5
  158.9 0.3 fusion.4
  160.0 0.0 copy-start.2
  160.1 0.0 copy-done
  160.1 1.5 convolution_convert_fusion
  161.6 0.0 copy-start.1
  161.6 14.5 %all-to-all-start.1 = ((bf16[8,32,2048]{2,1,0:T(8,128)(2,1)}), bf16[8,32,2048]{2,1,0:T(8,128)(2,1)S(1)}, u32[]{:S(2)}, u32[]{:S(2)}) async-start(bf16[8,32,2048]{2,1,0:T(8,128)(2,1)} %bitcast.21), calls=%async_computation.1 | async-start | bytes 2097152 | tf_op jit(solution)/shard_map/all_to_all | solution.py:59
  176.1 0.0 copy-done.2
  176.1 15.0 %all-to-all-done.1 = bf16[8,32,2048]{2,1,0:T(8,128)(2,1)S(1)} async-done(((bf16[8,32,2048]{2,1,0:T(8,128)(2,1)}), bf16[8,32,2048]{2,1,0:T(8,128)(2,1)S(1)}, u32[]{:S(2)}, u32[]{:S(2)}) %all-to-all-start.1) | async-done | bytes 1048608 | tf_op jit(solution)/shard_map/all_to_all | solution.py:59
  191.1 0.1 convert_reduce_fusion.1
  191.2 0.0 copy-done.1
  191.2 0.2 fusion.35
  191.4 0.1 fusion.37
  191.5 0.1 broadcast_in_dim.26
  191.6 18.3 %all_to_all.20 = bf16[8,32,2048]{2,1,0:T(8,128)(2,1)S(1)} all-to-all(bf16[8,32,2048]{2,1,0:T(8,128)(2,1)S(1)} %broadcast_in_dim.26), channel_id=1, replica_groups=mesh['sp'=64,'tp'=8] {'tp'}, dimensions={0} | all-to-all | bytes 2097152 | tf_op jit(solution)/shard_map/all_to_all | solution.py:27
  209.9 98.1 %all-gather.5.cloned.1.call-done = bf16[2048,2048]{1,0:T(8,128)(2,1)} async-done(((bf16[32,2048]{1,0:T(8,128)(2,1)}), bf16[2048,2048]{1,0:T(8,128)(2,1)}) %all-gather.5.cloned.1.call-update) | async-done | bytes 8388624 | tf_op jit(solution)/shard_map/all_gather | solution.py:15
  308.0 5.8 %fusion.20 = bf16[256,2048]{1,0:T(8,128)(2,1)S(1)} fusion(bf16[2048,2048]{1,0:T(8,128)(2,1)} %all-gather.5.cloned.1.call-done, bf16[256,2048]{1,0:T(8,128)(2,1)S(1)} %bitcast.57), kind=kOutput, calls=%fused_computation.29 | convolution fusion | flops 2148794368 | bytes 10485760 | tf_op jit(solution)/shard_map/dot_general | solution.py:145
  313.9 27.4 %all_to_all.21 = bf16[8,32,2048]{2,1,0:T(8,128)(2,1)S(1)} all-to-all(bf16[8,32,2048]{2,1,0:T(8,128)(2,1)S(1)} %bitcast.58), channel_id=1, replica_groups=mesh['sp'=64,'tp'=8] {'tp'}, dimensions={0} | all-to-all | bytes 2097152 | tf_op jit(solution)/shard_map/all_to_all | solution.py:59
  341.3 0.1 convert_reduce_fusion
  341.4 0.7 fusion.38
  (46 shorter events, 0.3 us)
Async XLA Ops:
  6.5 153.5 %copy-start = (bf16[128,2048]{1,0:T(8,128)(2,1)S(1)}, bf16[128,2048]{1,0:T(8,128)(2,1)}, u32[]{:S(2)}) copy-start(bf16[128,2048]{1,0:T(8,128)(2,1)} %param.22) | copy-start | bytes 1572868
  6.5 146.1 %all-gather.3.cloned.1.call-start = ((), (), s32[]{:S(2)}) async-start(), calls=%async_computation.4 | async-start | bytes 4259840 | tf_op jit(solution)/shard_map/all_gather | solution.py:49
  9.6 298.4 %all-gather.5.cloned.1.call-start = ((), (), s32[]{:S(2)}) async-start(), calls=%async_computation.5 | async-start | bytes 8519680 | tf_op jit(solution)/shard_map/all_gather | solution.py:15
  12.6 143.9 %all-to-all-start = ((f32[64,2,256]{2,1,0:T(2,128)}), f32[64,2,256]{2,1,0:T(2,128)S(1)}, u32[]{:S(2)}, u32[]{:S(2)}) async-start(f32[64,2,256]{2,1,0:T(2,128)} %broadcast_in_dim.25), calls=%async_computation | async-start | bytes 262144 | tf_op jit(solution)/shard_map/all_to_all | solution.py:27
  33.6 122.9 %copy-start.3 = (f32[2,256]{1,0:T(2,128)S(1)}, f32[2,256]{1,0:T(2,128)}, u32[]{:S(2)}) copy-start(f32[2,256]{1,0:T(2,128)} %param.19) | copy-start | bytes 6148
  160.0 16.1 %copy-start.2 = (bf16[2048]{0:T(1024)(128)(2,1)S(1)}, bf16[2048]{0:T(1024)(128)(2,1)}, u32[]{:S(2)}) copy-start(bf16[2048]{0:T(1024)(128)(2,1)} %param.23) | copy-start | bytes 12292
  161.6 29.6 %copy-start.1 = (bf16[32,2048]{1,0:T(8,128)(2,1)S(1)}, bf16[32,2048]{1,0:T(8,128)(2,1)}, u32[]{:S(2)}) copy-start(bf16[32,2048]{1,0:T(8,128)(2,1)} %param.15) | copy-start | bytes 393220
  161.6 29.5 %all-to-all-start.1 = ((bf16[8,32,2048]{2,1,0:T(8,128)(2,1)}), bf16[8,32,2048]{2,1,0:T(8,128)(2,1)S(1)}, u32[]{:S(2)}, u32[]{:S(2)}) async-start(bf16[8,32,2048]{2,1,0:T(8,128)(2,1)} %bitcast.21), calls=%async_computation.1 | async-start | bytes 2097152 | tf_op jit(solution)/shard_map/all_to_all | solution.py:59
Sparse Core Ops, SparseCore 0:
  10.2 142.3 all-gather.2
  155.6 152.4 all-gather.4
where the time goes:
time: 350 us; the launch traced here: 349 us
  waiting for transfers between devices  232 us (66%)
  blocking collectives  45.7 us (13%)
  starting transfers between devices  33.8 us (10%)
  between operations  13.6 us (4%)
  matrix products  9.29 us (3%)
  other arithmetic  7.18 us (2%)
  local copies, waits for them, and re-layouts  6.37 us (2%)
    all_gather x1, waiting for transfers between devices, in_one_piece(): lax.all_gather(both, axis, axis=dim, tiled=True)  119 us
    all_gather x1, waiting for transfers between devices, rows_first(): result = lax.all_gather(both, axis, axis=0, tiled=True)  98.1 us
    all_to_all x1, blocking collectives, summed_on_arrival(): parts = lax.all_to_all(cut_along(value, dim, count), axis, 0, 0, tiled=True)  27.4 us
    all_to_all x1, starting transfers between devices, sent_to_all(): lax.all_to_all(jnp.broadcast_to(value[None], (count, *value.shape)), axis...  19.3 us
    all_to_all x1, blocking collectives, sent_to_all(): lax.all_to_all(jnp.broadcast_to(value[None], (count, *value.shape)), axis...  18.3 us
    all_to_all x1, waiting for transfers between devices, summed_on_arrival(): parts = lax.all_to_all(cut_along(value, dim, count), axis, 0, 0, tiled=True)  15 us
    all_to_all x1, starting transfers between devices, summed_on_arrival(): parts = lax.all_to_all(cut_along(value, dim, count), axis, 0, 0, tiled=True)  14.5 us
  transfers between devices with their start and end apart: 4, of which 3 were waited for; matrix products, arithmetic and copies ran while one was open for 4% of the time, Pallas kernels for 0%

commit v1 on v0

v1 whole, which is shorter than its diff:
```python
import functools

import jax
import jax.numpy as jnp
from jax import lax
from jax.experimental import pallas as pl
from jax.experimental.pallas import tpu as pltpu
from jax.sharding import Mesh, PartitionSpec as P


EPS = 1e-06
NZ, NY, NX, NC = 16, 4, 4, 2
NTP = NX * NC
NK, NQ = 8, 8
PAIR = 2
MATES = PAIR * NTP
HEAD = 64
HEADS = 2
WIDE = HEADS * HEAD
TOK = 256
ROWS = 32
GATE = 16
KV_ROWS = 2 * HEAD + GATE
CHUNK = 4
PADS = CHUNK - 1
LOW = -1e30
F32 = jnp.float32
BF16 = jnp.bfloat16
VMEM = pl.BlockSpec(memory_space=pltpu.VMEM)
SMEM = pl.BlockSpec(memory_space=pltpu.SMEM)


def three_parts(value):
    high = value.astype(BF16).astype(F32)
    middle = (value - high).astype(BF16).astype(F32)
    low = (value - high - middle).astype(BF16).astype(F32)
    return [high, middle, low]


def parts_of_heads(rows):
    filler = jnp.zeros((GATE // HEADS - 3, TOK), F32)
    return jnp.concatenate([p for row in rows for p in (*three_parts(row), filler)], axis=0)


def prep_kernel(q_ref, k_ref, v_ref, gates_ref, qg_ref, kg_ref, up_ref, down_ref, q_out, kv_out, pair_out):
    half = up_ref.shape[1] // PAIR
    for n in range(NY):
        columns = slice((n % PAIR) * half, (n % PAIR + 1) * half)
        pair_out[n, 0] = up_ref[:, columns]
        pair_out[n, 1] = down_ref[:, columns]
    q = q_ref[...].astype(F32)
    halves = []
    for h in range(HEADS):
        part = q[:, h * HEAD : (h + 1) * HEAD]
        scale = lax.rsqrt(jnp.mean(part * part, axis=-1, keepdims=True) + EPS)
        halves.append(part * scale * qg_ref[...] * HEAD ** (-0.5))
    qn = jnp.concatenate(halves, axis=1).T.astype(BF16)
    for member in range(NQ):
        q_out[member] = qn
    row = lax.broadcasted_iota(jnp.int32, (HEAD, HEAD), 0)
    col = lax.broadcasted_iota(jnp.int32, (HEAD, HEAD), 1)
    k_gain = jnp.sum(jnp.where(row == col, kg_ref[...], 0.0), axis=1, keepdims=True)
    k = k_ref[...].astype(F32)
    scale = lax.rsqrt(jnp.mean(k * k, axis=0, keepdims=True) + EPS)
    kv_out[:HEAD] = (k * scale * k_gain).astype(BF16)
    kv_out[HEAD : HEAD + GATE] = parts_of_heads([-gates_ref[h : h + 1] for h in range(HEADS)]).astype(BF16)
    kv_out[HEAD + GATE :] = v_ref[...]


def attention_kernel(place_ref, q_ref, kv_ref, out_ref, keys_ref, vals_ref, qh_ref, m_ref, l_ref, acc_ref):
    slab = place_ref[0]
    member = place_ref[1]
    lane = lax.broadcasted_iota(jnp.int32, (TOK, WIDE), 1)
    nothing = jnp.where((lane == HEAD) | (lane == HEAD + GATE // HEADS), LOW, 0.0).astype(BF16)
    for j in range(PADS):
        keys_ref[j * TOK : (j + 1) * TOK] = nothing
    vals_ref[:, : PADS * TOK] = jnp.zeros((HEAD, PADS * TOK), BF16)
    rest = jnp.zeros((WIDE - HEAD - GATE, TOK), F32)
    for j in range(NK):
        rows = jnp.concatenate([kv_ref[j, : HEAD + GATE].astype(F32), rest], axis=0)
        where = slice((PADS + j) * TOK, (PADS + j + 1) * TOK)
        keys_ref[where] = rows.T.astype(BF16)
        vals_ref[:, where] = kv_ref[j, HEAD + GATE :]
    spot = lax.broadcasted_iota(jnp.int32, (WIDE - HEAD, TOK), 0)
    for h in range(HEADS):
        first = h * (GATE // HEADS)
        ones = jnp.where((spot >= first) & (spot < first + 3), 1.0, 0.0)
        qh_ref[HEAD:, h * TOK : (h + 1) * TOK] = ones.astype(BF16)

    def one_step(block, back, last):
        start = pl.multiple_of((slab - back * CHUNK) * TOK, TOK)
        s = jnp.dot(keys_ref[pl.ds(start, CHUNK * TOK)], qh_ref[...], preferred_element_type=F32)
        if last:
            key = lax.broadcasted_iota(jnp.int32, (TOK, HEADS * TOK), 0)
            query = lax.broadcasted_iota(jnp.int32, (TOK, HEADS * TOK), 1) & (TOK - 1)
            tail = jnp.where(key - query <= (block - member) * TOK, s[PADS * TOK :], LOW)
            s = jnp.concatenate([s[: PADS * TOK], tail], axis=0)
        new = jnp.max(s, axis=0, keepdims=True)
        if not last:
            old = m_ref[...]
            new = jnp.maximum(old, new)
            factor = jnp.exp(old - new)
        m_ref[...] = new
        p = jnp.exp(s - jnp.maximum(new, LOW * 0.5))
        total = jnp.sum(p, axis=0, keepdims=True)
        product = jnp.dot(vals_ref[:, pl.ds(start, CHUNK * TOK)], p.astype(BF16), preferred_element_type=F32)
        l_ref[...] = total if last else l_ref[...] * factor + total
        acc_ref[...] = product if last else acc_ref[...] * factor + product

    def one_block(block, carry):
        for h in range(HEADS):
            qh_ref[:HEAD, h * TOK : (h + 1) * TOK] = q_ref[block, h * HEAD : (h + 1) * HEAD]
        one_step(block, 0, True)

        def step(c, inner):
            one_step(block, c, False)
            return inner

        lax.fori_loop(1, slab // CHUNK + 1, step, 0)
        l = l_ref[...]
        some = l > 0.0
        safe = jnp.where(some, l, 1.0)
        out = (acc_ref[...] / safe).astype(BF16)
        lse = jnp.where(some, m_ref[...] + jnp.log(safe), LOW)
        for h in range(HEADS):
            out_ref[block, h * HEAD : (h + 1) * HEAD] = out[:, h * TOK : (h + 1) * TOK]
        rows = [lse[:, h * TOK : (h + 1) * TOK] for h in range(HEADS)]
        out_ref[block, WIDE:] = parts_of_heads(rows).astype(BF16)
        return carry

    lax.fori_loop(0, NQ, one_block, 0)


def merge_kernel(in_ref, out_ref):
    tails = [in_ref[n, WIDE:].astype(F32) for n in range(NQ)]
    halves = []
    for h in range(HEADS):
        a = h * (GATE // HEADS)
        sums = [t[a : a + 1] + t[a + 1 : a + 2] + t[a + 2 : a + 3] for t in tails]
        top = functools.reduce(jnp.maximum, sums)
        shares = [jnp.exp(v - top) for v in sums]
        denom = functools.reduce(jnp.add, shares)
        total = None
        for n in range(NQ):
            part = in_ref[n, h * HEAD : (h + 1) * HEAD].astype(F32) * shares[n]
            total = part if total is None else total + part
        halves.append(total / denom)
    attn = jnp.concatenate(halves, axis=0).T.astype(BF16)
    for n in range(MATES):
        out_ref[n] = attn


def ffn_kernel(
    place_ref, attn_ref, near_ref, far_ref, gain_ref, weight_ref,
    mixed_out, keep_out, send_out, total_ref, resid_ref, act_ref, up_ref, down_ref, sem,
):
    step = pl.program_id(0)
    x, core, mate = place_ref[0], place_ref[1], place_ref[2]
    span = weight_ref.shape[2]

    def copies(side):
        where = (up_ref, down_ref)[side]
        return [
            pltpu.make_async_copy(weight_ref.at[z, side], where.at[pl.ds(z * span, span)], sem.at[side, z])
            for z in range(NZ)
        ]

    @pl.when(step == 0)
    def _():
        for side in range(2):
            for copy in copies(side):
                copy.start()

    shift = jnp.where(step == 1, NX - 1, jnp.where(step == 2, 1, jnp.where(step == 3, 2, 0)))
    there = lax.rem(x + shift, NX)
    here = there * NC + core
    other = there * NC + (1 - core)
    right = jnp.concatenate([near_ref[0, :WIDE], far_ref[0, :WIDE]], axis=0)
    for t in range(PAIR):
        left = jnp.concatenate([attn_ref[t * NTP + here], attn_ref[t * NTP + other]], axis=1)
        part = jnp.dot(left, right, preferred_element_type=F32)
        rows = slice(t * TOK, (t + 1) * TOK)

        @pl.when(step == 0)
        def _():
            total_ref[rows] = part

        @pl.when(step > 0)
        def _():
            total_ref[rows] += part

    for source, index in ((near_ref, here), (far_ref, other)):
        for k in range(PAIR):
            token = jnp.where(k == 0, mate, 1 - mate)
            at = pl.multiple_of(token * TOK + index * ROWS, ROWS)
            resid_ref[pl.ds(at, ROWS)] = source[0, WIDE + k * ROWS : WIDE + (k + 1) * ROWS]

    @pl.when(step == NX - 1)
    def _():
        mixed = (resid_ref[...].astype(F32) + total_ref[...]).astype(BF16)
        resid_ref[...] = mixed
        own = pl.multiple_of(mate * TOK + (x * NC + core) * ROWS, ROWS)
        mixed_out[...] = resid_ref[pl.ds(own, ROWS)]
        wide = mixed.astype(F32)
        scale = lax.rsqrt(jnp.mean(wide * wide, axis=-1, keepdims=True) + EPS)
        normed = (wide * scale * gain_ref[...].astype(F32)).astype(BF16)
        for copy in copies(0):
            copy.wait()
        up = jnp.dot(normed, up_ref[...], preferred_element_type=F32)
        act_ref[...] = jnp.square(jnp.maximum(up, 0.0)).astype(BF16)
        for copy in copies(1):
            copy.wait()
        for out, side in ((send_out, 1 - core), (keep_out, core)):
            pieces = []
            for t in range(PAIR):
                for n in range(NX):
                    at = pl.multiple_of(t * TOK + n * NC * ROWS + side * ROWS, ROWS)
                    pieces.append(act_ref[pl.ds(at, ROWS)])
            out[...] = lax.dot_general(
                jnp.concatenate(pieces, axis=0), down_ref[...], (((1,), (1,)), ((), ())), preferred_element_type=F32
            ).astype(BF16)


def call(kernel, shapes, smem=0, count=0, scratch=()):
    return pl.pallas_call(
        kernel,
        out_shape=shapes,
        in_specs=[SMEM] * smem + [VMEM] * count,
        out_specs=jax.tree.map(lambda _: VMEM, shapes),
        scratch_shapes=list(scratch),
    )


def attention(place, q_all, kv):
    return call(
        attention_kernel,
        jax.ShapeDtypeStruct((NQ, KV_ROWS, TOK), BF16),
        smem=1,
        count=2,
        scratch=(
            pltpu.VMEM(((NK + PADS) * TOK, WIDE), BF16),
            pltpu.VMEM((HEAD, (NK + PADS) * TOK), BF16),
            pltpu.VMEM((WIDE, HEADS * TOK), BF16),
            pltpu.VMEM((1, HEADS * TOK), F32),
            pltpu.VMEM((1, HEADS * TOK), F32),
            pltpu.VMEM((HEAD, HEADS * TOK), F32),
        ),
    )(place, q_all, kv)


def ffn(place, attn_all, near, far, gain, weights):
    model = near.shape[2]
    width = weights.shape[3]
    around = pl.BlockSpec((1, near.shape[1], model), lambda r: (r, 0, 0))
    return pl.pallas_call(
        ffn_kernel,
        grid=(NX,),
        out_shape=(jax.ShapeDtypeStruct((ROWS, model), BF16), *[jax.ShapeDtypeStruct((TOK, model), BF16)] * 2),
        in_specs=[SMEM, VMEM, around, around, VMEM, pl.BlockSpec(memory_space=pl.ANY)],
        out_specs=(VMEM, VMEM, VMEM),
        scratch_shapes=[
            pltpu.VMEM((PAIR * TOK, model), F32),
            pltpu.VMEM((PAIR * TOK, model), BF16),
            pltpu.VMEM((PAIR * TOK, width), BF16),
            pltpu.VMEM((model, width), BF16),
            pltpu.VMEM((model, width), BF16),
            pltpu.SemaphoreType.DMA((2, NZ)),
        ],
        name="ffn",
    )(place, attn_all, near, far, gain, weights)


def ring(count, step):
    return [(i, (i + step) % count) for i in range(count)]


def inside(resid, queries, keys, values, log_gates, q_gain, k_gain, w_out, mlp_gain, w_up, w_down):
    model = resid.shape[1]
    half = w_up.shape[1] // PAIR
    columns = ("yh", "yl")
    members = ("zq", *columns)
    mates = ("yl", "x", "c")

    theirs = lax.ppermute(resid, "yl", ring(PAIR, 1))
    q_sent, kv_sent, pair = call(
        prep_kernel,
        (
            jax.ShapeDtypeStruct((NQ, WIDE, TOK), BF16),
            jax.ShapeDtypeStruct((KV_ROWS, TOK), BF16),
            jax.ShapeDtypeStruct((NY, 2, ROWS, half), BF16),
        ),
        count=8,
    )(queries, keys, values, log_gates, q_gain.reshape(1, HEAD), k_gain.reshape(1, HEAD), w_up, w_down.T)
    pair = lax.all_to_all(pair, columns, 0, 0, tiled=True)
    pair = jnp.moveaxis(pair, 0, 1).reshape(1, 2, NY * ROWS, half)
    weights = lax.all_gather(pair, ("zp", "zq"), axis=0, tiled=True)

    own = jnp.concatenate([w_out, resid, theirs], axis=0)
    arrived = [own]
    for step in (1, -1, 2):
        arrived.append(lax.ppermute(own, "x", ring(NX, step)))
    near = jnp.stack(arrived, axis=0)
    far = lax.ppermute(near, "c", ring(NC, 1))

    q_all = lax.all_to_all(q_sent, members, 0, 0, tiled=True)
    kv = lax.all_gather(kv_sent[None], "zp", axis=0, tiled=True)

    place = jnp.stack([lax.axis_index("zp"), lax.axis_index(members)]).astype(jnp.int32)
    partial = attention(place, q_all, kv)
    partial = lax.all_to_all(partial, members, 0, 0, tiled=True)
    attn = call(merge_kernel, jax.ShapeDtypeStruct((MATES, TOK, WIDE), BF16), count=1)(partial)
    attn_all = lax.all_to_all(attn, mates, 0, 0, tiled=True)
    spot = jnp.stack([lax.axis_index("x"), lax.axis_index("c"), lax.axis_index("yl")]).astype(jnp.int32)
    mixed, keep, send = ffn(spot, attn_all, near, far, mlp_gain.reshape(1, model), weights)
    got = lax.ppermute(send, "c", ring(NC, 1))
    both = (keep.astype(F32) + got.astype(F32)).astype(BF16)
    parts = lax.all_to_all(both.reshape(PAIR * NX, ROWS, model), ("yl", "x"), 0, 0, tiled=True)
    return (mixed.astype(F32) + jnp.sum(parts.astype(F32), axis=0)).astype(BF16)


def solution(mesh):
    fine = Mesh(
        mesh.devices.reshape(NK, NZ // NK, NY // PAIR, PAIR, NX, NC), ("zp", "zq", "yh", "yl", "x", "c")
    )
    sp, tp = ("zp", "zq", "yh", "yl"), ("x", "c")
    return jax.shard_map(
        inside,
        mesh=fine,
        in_specs=(
            P((*sp, *tp), None),
            P(sp, tp),
            P(tp, sp),
            P(tp, sp),
            P(tp, sp),
            P(),
            P(),
            P(tp, None),
            P(),
            P(sp, tp),
            P(tp, sp),
        ),
        out_specs=P((*sp, *tp), None),
        check_vma=False,
    )
```

time: 350 us -> 187 us (0.53)
  waiting for transfers between devices: 232 us -> 17.2 us
  blocking collectives: 45.7 us -> 81.8 us
  Pallas kernels: 0 us -> 28.7 us
  matrix products: 9.29 us -> 0 us
    all_gather x2 -> x1, waiting for transfers between devices: 217 us -> 0.01 us  [inside(): weights = lax.all_gather(pair, ('zp', 'zq'), axis=0, tiled=True)]
    all_gather x0 -> x1, blocking collectives: none -> 36.3 us  [inside(): kv = lax.all_gather(kv_sent[None], 'zp', axis=0, tiled=True)]
    pallas_call x0 -> x4, Pallas kernels: none -> 28.7 us  [the longest x1 13 us: ffn(): pl.pallas_call(ffn_kernel, grid=(NX,), out_shape=(jax.ShapeDtypeStruct((R...]
    ppermute x0 -> x6, starting transfers between devices: none -> 24.4 us  [the longest x3 9.93 us: inside(): arrived.append(lax.ppermute(own, 'x', ring(NX, step)))]
    all_to_all x2, starting transfers between devices: 33.8 us -> 9.96 us  [the longest x1 5.53 us: inside(): attn_all = lax.all_to_all(attn, mates, 0, 0, tiled=True)]
    dot_general x4 -> x0, matrix products: 9.29 us -> none  [the longest x1 5.81 us: local(): jnp.dot(rows_now, down_whole, preferred_element_type=jnp.float32)]
    all_to_all x2 -> x3, blocking collectives: 45.7 us -> 45.5 us  [the longest x1 18.3 us: inside(): lax.all_to_all(both.reshape(PAIR * NX, ROWS, model), ('yl', 'x'), 0, 0, t...]
  transfers between devices with their start and end apart: 4 -> 9, of which waited for: 3 -> 2; matrix products, arithmetic and copies ran while one was open for 4% -> 3% of each run, Pallas kernels for 0% -> 7%
where the time goes in v1:
time: 187 us; the launch traced here: 185 us
  blocking collectives  81.8 us (44%)
  starting transfers between devices  34.4 us (18%)
  Pallas kernels  28.7 us (15%)
  waiting for transfers between devices  17.2 us (9%)
  between operations  13.6 us (7%)
  other arithmetic  5.81 us (3%)
  local copies, waits for them, and re-layouts  3.89 us (2%)
    all_gather x1, blocking collectives, inside(): kv = lax.all_gather(kv_sent[None], 'zp', axis=0, tiled=True)  36.3 us
    all_to_all x1, blocking collectives, inside(): lax.all_to_all(both.reshape(PAIR * NX, ROWS, model), ('yl', 'x'), 0, 0, t...  18.3 us
    all_to_all x1, blocking collectives, inside(): partial = lax.all_to_all(partial, members, 0, 0, tiled=True)  16.6 us
    all_to_all x1, waiting for transfers between devices, inside(): attn_all = lax.all_to_all(attn, mates, 0, 0, tiled=True)  14.7 us
    pallas_call x1, Pallas kernels, ffn(): pl.pallas_call(ffn_kernel, grid=(NX,), out_shape=(jax.ShapeDtypeStruct((R...  13 us
    pallas_call x1, Pallas kernels, attention(): call(attention_kernel, jax.ShapeDtypeStruct((NQ, KV_ROWS, TOK), BF16), sm...  11.1 us
    all_to_all x1, blocking collectives, inside(): pair = lax.all_to_all(pair, columns, 0, 0, tiled=True)  10.7 us
    ppermute x3, starting transfers between devices, inside(): arrived.append(lax.ppermute(own, 'x', ring(NX, step)))  9.93 us
  transfers between devices with their start and end apart: 9, of which 2 were waited for; matrix products, arithmetic and copies ran while one was open for 3% of the time, Pallas kernels for 7%

profile of v1, /device:TPU:1, one launch (start us, length us, event | category | flops | bytes accessed | tf_op | source)
XLA Modules:
  0.0 185.4 jit_solution(7941487346723470793)
XLA Ops:
  6.5 0.0 copy-start.5
  6.5 0.0 all-gather.3.cloned.1.call-start
  6.5 2.2 %shard_map.109 = (bf16[8,128,256]{2,1,0:T(8,128)(2,1)}, bf16[144,256]{1,0:T(8,128)(2,1)}, bf16[4,2,32,512]{3,2,1,0:T(8,128)(2,1)}) custom-call(bf16[256,128]{1,0:T(8,128)(2,1)} %q_ref.1, bf16[64,256]{1,0:T(8,128)(2,1)} %k_ref.1, bf16[64,256]{1,0:T(8,128)(2,1)} %v_ref.1, f32[2,256]{1,0:T(2,128)} %gates_ref.1, f32[1,64]{1,0:T(1,128)} %bitcast.25, ...), custom_call_target="tpu_custom_call" | custom-call | tf_op jit(solution)/shard_map/pallas_call | solution.py:285
  8.7 0.0 copy-start.7
  8.7 10.7 %all_to_all.25 = bf16[4,2,32,512]{3,2,1,0:T(8,128)(2,1)S(1)} all-to-all(bf16[4,2,32,512]{3,2,1,0:T(8,128)(2,1)} %get-tuple-element.13), channel_id=1, replica_groups=mesh['zp'=8,'zq'=2,'yh'=2,'yl'=2,'x'=4,'c'=2] {'yh','yl'}, dimensions={0} | all-to-all | bytes 524288 | tf_op jit(solution)/shard_map/all_to_all | solution.py:294
  19.4 0.8 copy.13
  20.2 0.0 all-gather.3.cloned.1.call-update
  20.2 2.2 %collective-permute-start = (bf16[32,2048]{1,0:T(8,128)(2,1)}, bf16[32,2048]{1,0:T(8,128)(2,1)S(1)}, u32[]{:S(2)}, u32[]{:S(2)}) collective-permute-start(bf16[32,2048]{1,0:T(8,128)(2,1)} %param.11), channel_id=1, source_target_pairs={{0,8},{8,0},{1,9},{9,1},{2,10},{10,2},{3,11},{11,3},{4,12},{12,4},... | collective-permute-start | bytes 393224 | tf_op jit(solution)/shard_map/ppermute | solution.py:284
  22.4 4.4 %all-to-all-start = ((bf16[8,128,256]{2,1,0:T(8,128)(2,1)}), bf16[8,128,256]{2,1,0:T(8,128)(2,1)}, u32[]{:S(2)}, u32[]{:S(2)}) async-start(bf16[8,128,256]{2,1,0:T(8,128)(2,1)} %get-tuple-element.11), calls=%async_computation | async-start | bytes 1048576 | tf_op jit(solution)/shard_map/all_to_all | solution.py:305
  26.8 1.1 constant_dynamic-update-slice_fusion.2
  27.9 0.0 copy-done.5
  27.9 0.0 collective-permute-done
  28.0 0.0 copy-start.1
  28.0 4.7 %collective-permute-start.3 = (bf16[192,2048]{1,0:T(8,128)(2,1)S(1)}, bf16[192,2048]{1,0:T(8,128)(2,1)S(1)}, u32[]{:S(2)}, u32[]{:S(2)}) collective-permute-start(bf16[192,2048]{1,0:T(8,128)(2,1)S(1)} %constant_dynamic-update-slice_fusion), channel_id=1, source_target_pairs={{0,4},{2,6},{4,0},{6,2},{1,5},{3,7},{5,1},{7,3},{8,12},{10,14},{12... | collective-permute-start | bytes 2359304 | tf_op jit(solution)/shard_map/ppermute | solution.py:301
  32.6 2.8 %collective-permute-start.2 = (bf16[192,2048]{1,0:T(8,128)(2,1)S(1)}, bf16[192,2048]{1,0:T(8,128)(2,1)S(1)}, u32[]{:S(2)}, u32[]{:S(2)}) collective-permute-start(bf16[192,2048]{1,0:T(8,128)(2,1)S(1)} %constant_dynamic-update-slice_fusion), channel_id=1, source_target_pairs={{0,6},{2,0},{4,2},{6,4},{1,7},{3,1},{5,3},{7,5},{8,14},{10,8},{12,... | collective-permute-start | bytes 2359304 | tf_op jit(solution)/shard_map/ppermute | solution.py:301
  35.4 2.5 %collective-permute-start.1 = (bf16[192,2048]{1,0:T(8,128)(2,1)S(1)}, bf16[192,2048]{1,0:T(8,128)(2,1)S(1)}, u32[]{:S(2)}, u32[]{:S(2)}) collective-permute-start(bf16[192,2048]{1,0:T(8,128)(2,1)S(1)} %constant_dynamic-update-slice_fusion), channel_id=1, source_target_pairs={{0,2},{2,4},{4,6},{6,0},{1,3},{3,5},{5,7},{7,1},{8,10},{10,12},{12... | collective-permute-start | bytes 2359304 | tf_op jit(solution)/shard_map/ppermute | solution.py:301
  37.9 0.0 copy-done.7
  37.9 36.3 %all-gather = bf16[1152,256]{1,0:T(8,128)(2,1)} all-gather(bf16[144,256]{1,0:T(8,128)(2,1)S(1)} %copy-done.7), channel_id=2, replica_groups=mesh['zp'=8,'zq'=2,'yh'=2,'yl'=2,'x'=4,'c'=2] {'zp'}, dimensions={0}, use_global_device_ids=true | all-gather | bytes 663552 | tf_op jit(solution)/shard_map/all_gather | solution.py:306
  74.3 0.0 collective-permute-done.3
  74.3 0.0 copy-start.2
  74.3 0.0 collective-permute-done.2
  74.3 0.0 copy-start.3
  74.3 0.0 collective-permute-done.1
  74.3 0.0 copy-start.4
  74.3 0.0 copy-done.1
  74.3 0.9 copy-done.2
  75.2 0.3 copy-done.3
  75.5 0.2 copy-done.4
  75.7 2.1 %pad_maximum_fusion.near_ref = bf16[4,192,2048]{2,1,0:T(8,128)(2,1)S(1)} fusion(bf16[1,192,2048]{2,1,0:T(8,128)(2,1)} %bitcast.21, bf16[1,192,2048]{2,1,0:T(8,128)(2,1)} %bitcast.22, bf16[1,192,2048]{2,1,0:T(8,128)(2,1)} %bitcast.23, bf16[1,192,2048]{2,1,0:T(8,128)(2,1)} %bitcast.18), kind=kLoop, calls=%fused_computation | loop fusion | flops 4718592 | bytes 6291456 | tf_op jit(solution)/shard_map/stack | solution.py:302
  77.8 0.0 copy-start
  77.8 9.6 %collective-permute-start.4 = (bf16[4,192,2048]{2,1,0:T(8,128)(2,1)S(1)}, bf16[4,192,2048]{2,1,0:T(8,128)(2,1)}, u32[]{:S(2)}, u32[]{:S(2)}) collective-permute-start(bf16[4,192,2048]{2,1,0:T(8,128)(2,1)S(1)} %pad_maximum_fusion.near_ref), channel_id=1, source_target_pairs={{0,1},{1,0},{2,3},{3,2},{4,5},{5,4},{6,7},{7,6},{8,9},{9,8},{10,11... | collective-permute-start | bytes 9437192 | tf_op jit(solution)/shard_map/ppermute | solution.py:303
  87.4 0.6 pad_add_fusion.1.place_ref
  88.0 0.0 all-to-all-done.q_ref
  88.0 0.0 copy-start.8
  88.0 11.1 %shard_map.110 = bf16[8,144,256]{2,1,0:T(8,128)(2,1)} custom-call(s32[2]{0:T(128)} %pad_add_fusion.1.place_ref, bf16[8,128,256]{2,1,0:T(8,128)(2,1)} %all-to-all-done.q_ref, bf16[8,144,256]{2,1,0:T(8,128)(2,1)} %bitcast.17), custom_call_target="tpu_custom_call" | custom-call | tf_op jit(solution)/shard_map/pallas_call | solution.py:235
  99.1 16.6 %all_to_all.26.in_ref = bf16[8,144,256]{2,1,0:T(8,128)(2,1)} all-to-all(bf16[8,144,256]{2,1,0:T(8,128)(2,1)} %shard_map.110), channel_id=1, replica_groups=mesh['zp'=8,'zq'=2,'yh'=2,'yl'=2,'x'=4,'c'=2] {'zq','yh','yl'}, dimensions={0} | all-to-all | bytes 1179648 | tf_op jit(solution)/shard_map/all_to_all | solution.py:310
  115.7 2.4 %shard_map.111 = bf16[16,256,128]{2,1,0:T(8,128)(2,1)} custom-call(bf16[8,144,256]{2,1,0:T(8,128)(2,1)} %all_to_all.26.in_ref), custom_call_target="tpu_custom_call" | custom-call | tf_op jit(solution)/shard_map/pallas_call | solution.py:311
  118.1 0.0 copy-done
  118.1 5.5 %all-to-all-start.2 = ((bf16[16,256,128]{2,1,0:T(8,128)(2,1)}), bf16[16,256,128]{2,1,0:T(8,128)(2,1)}, u32[]{:S(2)}, u32[]{:S(2)}) async-start(bf16[16,256,128]{2,1,0:T(8,128)(2,1)} %shard_map.111), calls=%async_computation.2 | async-start | bytes 2097152 | tf_op jit(solution)/shard_map/all_to_all | solution.py:312
  123.6 0.0 copy-done.8
  123.6 0.6 reshape.17.gain_ref
  124.2 0.7 pad_add_fusion.place_ref
  124.9 0.0 collective-permute-done.4.far_ref
  124.9 14.7 %all-to-all-done.2.attn_ref = bf16[16,256,128]{2,1,0:T(8,128)(2,1)} async-done(((bf16[16,256,128]{2,1,0:T(8,128)(2,1)}), bf16[16,256,128]{2,1,0:T(8,128)(2,1)}, u32[]{:S(2)}, u32[]{:S(2)}) %all-to-all-start.2) | async-done | bytes 1048608 | tf_op jit(solution)/shard_map/all_to_all | solution.py:312
  139.6 0.0 all-gather.3.cloned.1.call-done.weight_ref
  139.6 13.0 %ffn.1 = (bf16[32,2048]{1,0:T(8,128)(2,1)}, bf16[256,2048]{1,0:T(8,128)(2,1)}, bf16[256,2048]{1,0:T(8,128)(2,1)}) custom-call(s32[3]{0:T(128)} %pad_add_fusion.place_ref, bf16[16,256,128]{2,1,0:T(8,128)(2,1)} %all-to-all-done.2.attn_ref, bf16[4,192,2048]{2,1,0:T(8,128)(2,1)} %copy-done, bf16[4,192,2048]{2,1,0:T(8,128)(2,1)} %collective-permute-done.4.far_ref, ...), custom_call_target="tpu_custom_call" | custom-call | tf_op jit(solution)/shard_map/ffn/pallas_call | solution.py:255
  152.6 2.7 %collective-permute-start.5 = (bf16[256,2048]{1,0:T(8,128)(2,1)}, bf16[256,2048]{1,0:T(8,128)(2,1)S(1)}, u32[]{:S(2)}, u32[]{:S(2)}) collective-permute-start(bf16[256,2048]{1,0:T(8,128)(2,1)} %get-tuple-element.16), channel_id=1, source_target_pairs={{0,1},{1,0},{2,3},{3,2},{4,5},{5,4},{6,7},{7,6},{8,9},{9,8},{10,11... | collective-permute-start | bytes 3145736 | tf_op jit(solution)/shard_map/ppermute | solution.py:315
  155.3 2.5 %collective-permute-done.5 = bf16[256,2048]{1,0:T(8,128)(2,1)S(1)} collective-permute-done((bf16[256,2048]{1,0:T(8,128)(2,1)}, bf16[256,2048]{1,0:T(8,128)(2,1)S(1)}, u32[]{:S(2)}, u32[]{:S(2)}) %collective-permute-start.5) | collective-permute-done | bytes 1048608 | tf_op jit(solution)/shard_map/ppermute | solution.py:315
  157.8 0.0 copy-start.6
  157.8 1.6 add_convert_fusion
  159.4 18.3 %all_to_all.27 = bf16[8,32,2048]{2,1,0:T(8,128)(2,1)S(1)} all-to-all(bf16[8,32,2048]{2,1,0:T(8,128)(2,1)S(1)} %bitcast.16), channel_id=1, replica_groups=mesh['zp'=8,'zq'=2,'yh'=2,'yl'=2,'x'=4,'c'=2] {'yl','x'}, dimensions={0} | all-to-all | bytes 2097152 | tf_op jit(solution)/shard_map/all_to_all | solution.py:317
  177.7 0.1 convert_reduce_fusion
  177.9 0.0 copy-done.6
  177.9 0.7 add_convert_fusion.1
  (2 shorter events, 0.0 us)
Async XLA Ops:
  6.5 21.4 %copy-start.5 = (bf16[32,2048]{1,0:T(8,128)(2,1)S(1)}, bf16[32,2048]{1,0:T(8,128)(2,1)}, u32[]{:S(2)}) copy-start(bf16[32,2048]{1,0:T(8,128)(2,1)} %param.11) | copy-start | bytes 393220
  6.5 133.1 %all-gather.3.cloned.1.call-start = ((), (), s32[]{:S(2)}) async-start(), calls=%async_computation.5 | async-start | bytes 4456448 | tf_op jit(solution)/shard_map/all_gather | solution.py:296
  8.7 29.2 %copy-start.7 = (bf16[144,256]{1,0:T(8,128)(2,1)S(1)}, bf16[144,256]{1,0:T(8,128)(2,1)}, u32[]{:S(2)}) copy-start(bf16[144,256]{1,0:T(8,128)(2,1)} %get-tuple-element.12) | copy-start | bytes 221188
  20.2 7.7 %collective-permute-start = (bf16[32,2048]{1,0:T(8,128)(2,1)}, bf16[32,2048]{1,0:T(8,128)(2,1)S(1)}, u32[]{:S(2)}, u32[]{:S(2)}) collective-permute-start(bf16[32,2048]{1,0:T(8,128)(2,1)} %param.11), channel_id=1, source_target_pairs={{0,8},{8,0},{1,9},{9,1},{2,10},{10,2},{3,11},{11,3},{4,12},{12,4},... | collective-permute-start | bytes 393224 | tf_op jit(solution)/shard_map/ppermute | solution.py:284
  22.4 65.6 %all-to-all-start = ((bf16[8,128,256]{2,1,0:T(8,128)(2,1)}), bf16[8,128,256]{2,1,0:T(8,128)(2,1)}, u32[]{:S(2)}, u32[]{:S(2)}) async-start(bf16[8,128,256]{2,1,0:T(8,128)(2,1)} %get-tuple-element.11), calls=%async_computation | async-start | bytes 1048576 | tf_op jit(solution)/shard_map/all_to_all | solution.py:305
  28.0 46.3 %copy-start.1 = (bf16[192,2048]{1,0:T(8,128)(2,1)}, bf16[192,2048]{1,0:T(8,128)(2,1)S(1)}, u32[]{:S(2)}) copy-start(bf16[192,2048]{1,0:T(8,128)(2,1)S(1)} %constant_dynamic-update-slice_fusion) | copy-start | bytes 2359300
  28.0 46.3 %collective-permute-start.3 = (bf16[192,2048]{1,0:T(8,128)(2,1)S(1)}, bf16[192,2048]{1,0:T(8,128)(2,1)S(1)}, u32[]{:S(2)}, u32[]{:S(2)}) collective-permute-start(bf16[192,2048]{1,0:T(8,128)(2,1)S(1)} %constant_dynamic-update-slice_fusion), channel_id=1, source_target_pairs={{0,4},{2,6},{4,0},{6,2},{1,5},{3,7},{5,1},{7,3},{8,12},{10,14},{12... | collective-permute-start | bytes 2359304 | tf_op jit(solution)/shard_map/ppermute | solution.py:301
  32.6 41.6 %collective-permute-start.2 = (bf16[192,2048]{1,0:T(8,128)(2,1)S(1)}, bf16[192,2048]{1,0:T(8,128)(2,1)S(1)}, u32[]{:S(2)}, u32[]{:S(2)}) collective-permute-start(bf16[192,2048]{1,0:T(8,128)(2,1)S(1)} %constant_dynamic-update-slice_fusion), channel_id=1, source_target_pairs={{0,6},{2,0},{4,2},{6,4},{1,7},{3,1},{5,3},{7,5},{8,14},{10,8},{12,... | collective-permute-start | bytes 2359304 | tf_op jit(solution)/shard_map/ppermute | solution.py:301
  35.4 38.9 %collective-permute-start.1 = (bf16[192,2048]{1,0:T(8,128)(2,1)S(1)}, bf16[192,2048]{1,0:T(8,128)(2,1)S(1)}, u32[]{:S(2)}, u32[]{:S(2)}) collective-permute-start(bf16[192,2048]{1,0:T(8,128)(2,1)S(1)} %constant_dynamic-update-slice_fusion), channel_id=1, source_target_pairs={{0,2},{2,4},{4,6},{6,0},{1,3},{3,5},{5,7},{7,1},{8,10},{10,12},{12... | collective-permute-start | bytes 2359304 | tf_op jit(solution)/shard_map/ppermute | solution.py:301
  74.3 0.9 copy-start.2
  74.3 1.2 copy-start.3
  74.3 1.4 copy-start.4
  77.8 40.3 %copy-start = (bf16[4,192,2048]{2,1,0:T(8,128)(2,1)}, bf16[4,192,2048]{2,1,0:T(8,128)(2,1)S(1)}, u32[]{:S(2)}) copy-start(bf16[4,192,2048]{2,1,0:T(8,128)(2,1)S(1)} %pad_maximum_fusion.near_ref) | copy-start | bytes 9437188
  77.8 47.1 %collective-permute-start.4 = (bf16[4,192,2048]{2,1,0:T(8,128)(2,1)S(1)}, bf16[4,192,2048]{2,1,0:T(8,128)(2,1)}, u32[]{:S(2)}, u32[]{:S(2)}) collective-permute-start(bf16[4,192,2048]{2,1,0:T(8,128)(2,1)S(1)} %pad_maximum_fusion.near_ref), channel_id=1, source_target_pairs={{0,1},{1,0},{2,3},{3,2},{4,5},{5,4},{6,7},{7,6},{8,9},{9,8},{10,11... | collective-permute-start | bytes 9437192 | tf_op jit(solution)/shard_map/ppermute | solution.py:303
  88.0 35.6 %copy-start.8 = (bf16[2048]{0:T(1024)(128)(2,1)S(1)}, bf16[2048]{0:T(1024)(128)(2,1)}, u32[]{:S(2)}) copy-start(bf16[2048]{0:T(1024)(128)(2,1)} %param.19) | copy-start | bytes 12292
  118.1 21.5 %all-to-all-start.2 = ((bf16[16,256,128]{2,1,0:T(8,128)(2,1)}), bf16[16,256,128]{2,1,0:T(8,128)(2,1)}, u32[]{:S(2)}, u32[]{:S(2)}) async-start(bf16[16,256,128]{2,1,0:T(8,128)(2,1)} %shard_map.111), calls=%async_computation.2 | async-start | bytes 2097152 | tf_op jit(solution)/shard_map/all_to_all | solution.py:312
  152.6 5.2 %collective-permute-start.5 = (bf16[256,2048]{1,0:T(8,128)(2,1)}, bf16[256,2048]{1,0:T(8,128)(2,1)S(1)}, u32[]{:S(2)}, u32[]{:S(2)}) collective-permute-start(bf16[256,2048]{1,0:T(8,128)(2,1)} %get-tuple-element.16), channel_id=1, source_target_pairs={{0,1},{1,0},{2,3},{3,2},{4,5},{5,4},{6,7},{7,6},{8,9},{9,8},{10,11... | collective-permute-start | bytes 3145736 | tf_op jit(solution)/shard_map/ppermute | solution.py:315
  157.8 20.1 %copy-start.6 = (bf16[32,2048]{1,0:T(8,128)(2,1)S(1)}, bf16[32,2048]{1,0:T(8,128)(2,1)}, u32[]{:S(2)}) copy-start(bf16[32,2048]{1,0:T(8,128)(2,1)} %get-tuple-element.14) | copy-start | bytes 393220
Sparse Core Ops, SparseCore 0:
  20.3 81.5 all-gather.2
